TPU v7x, 32 devices: a whole 2x2x4 slice. The times are simulated.
32 devices in a mesh: sp: 8 (over z, core), tp: 4 (over y, x).
Axes of the slice: x: 2, y: 2, z: 4, core: 2. Of those that a mesh axis runs over, the one named last changes fastest.
Arguments:
- outer_gate: bfloat16 [2048, 1024], P('sp', 'tp'), may hold values from -6 to 6
- inner_gate: bfloat16 [2048, 1024], P('sp', 'tp'), may hold values from -6 to 6
- values: bfloat16 [2048, 1024], P('sp', 'tp'), may hold values from -6 to 6
- conv_taps: bfloat16 [3, 1024], P(None, 'tp'), may hold values from -3.5 to 3.5
- document: int32 [2048], P('sp'), may hold values from 0 to 3, never falling along the last dimension, each value on 1 to 1024 neighbouring positions
- mix_proj: bfloat16 [1024, 2048], P('tp'), may hold values from -0.1875 to 0.1875
- stream: bfloat16 [2048, 2048], P('sp'), may hold values from -6 to 6
- norm_gain: float32 [2048], replicated, may hold values from 0.1 to 1.9
- routes: int32 [2048, 2], P('sp'), may hold values from 0 to 7, all different within a row; in each aligned block of 256 rows (0 to 255, 256 to 511, ...) at most 96 rows name the same one
- route_weight: float32 [2048, 2], P('sp'), may hold values from 0.25 to 1
- w_gate: bfloat16 [8, 2048, 4096], P('sp', None, 'tp'), may hold values from -0.125 to 0.125
- w_up: bfloat16 [8, 2048, 4096], P('sp', None, 'tp'), may hold values from -0.125 to 0.125
- w_down: bfloat16 [8, 4096, 2048], P('sp', 'tp'), may hold values from -0.09375 to 0.09375
Outputs:
- mixed: bfloat16 [2048, 2048], P('sp', 'tp')
Inputs may be any that keep to these rules, and one draw needn't show every extreme that they name: Document numbers never fall along the sequence; each document holds 1 to 1024 consecutive tokens and one holds exactly that many. `routes`: each token names 2 different experts. Among the 256 tokens of one sp index no expert is named by more than 96 tokens, and in some sp index's tokens an expert is named by exactly 96.
All inputs are finite; a program needn't handle non-finite values.
Results may differ from a plain program's by a relative error of at most 0.014.
Values may be sent and summed in bfloat16 or wider, within the bound.
A program may use at most 64 MiB of HBM per device.

v0:
```python
import jax
import jax.numpy as jnp
from jax import lax
from jax.sharding import PartitionSpec as P


def passed_along(value, axis, steps):
    count = lax.axis_size(axis)
    first, last = (max(0, -steps), min(count, count - steps))
    return lax.ppermute(value, axis, [(source, source + steps) for source in range(first, last)])


def finish(gate, upper, w_down):
    act = (jax.nn.silu(gate) * upper).astype(jnp.bfloat16)
    partial_value = jnp.dot(act, w_down[0], preferred_element_type=jnp.float32)
    return lax.psum_scatter(
        partial_value.astype(jnp.bfloat16), "tp", scatter_dimension=1, tiled=True
    )


def body(
    outer_gate,
    inner_gate,
    values,
    conv_taps,
    document,
    mix_proj,
    stream,
    norm_gain,
    routes,
    route_weight,
    w_gate,
    w_up,
    w_down,
):
    length = stream.shape[0]
    features = stream.shape[1]
    groups = lax.axis_size("sp")
    capacity = 3 * length // groups
    chosen_count = routes.shape[1]
    width = features // lax.axis_size("tp")
    column = lax.axis_index("tp") * width
    product = inner_gate.astype(jnp.float32) * values.astype(jnp.float32)
    doc_float = document.astype(jnp.float32)
    rim_values, rim_docs = passed_along((product[-2:], doc_float[-2:]), "sp", 1)
    padded_values = jnp.concatenate([rim_values, product], axis=0)
    padded_docs = jnp.concatenate([rim_docs, doc_float], axis=0)
    kernel = conv_taps.astype(jnp.float32)
    conv = kernel[2] * product
    for back in (1, 2):
        offset = 2 - back
        same = (padded_docs[offset : offset + length] == doc_float)[:, None]
        conv = conv + kernel[offset] * jnp.where(same, padded_values[offset : offset + length], 0.0)
    gated = (outer_gate.astype(jnp.float32) * conv).astype(jnp.bfloat16)
    partial_value = jnp.dot(gated, mix_proj, preferred_element_type=jnp.float32)
    hidden_state = stream.astype(jnp.float32) + lax.psum(
        partial_value.astype(jnp.bfloat16), "tp"
    ).astype(jnp.float32)
    scale = lax.rsqrt(jnp.mean(hidden_state * hidden_state, axis=-1, keepdims=True) + 1e-06)
    normed = (hidden_state * scale * norm_gain).astype(jnp.bfloat16)
    own_part = lax.dynamic_slice_in_dim(hidden_state, column, width, 1)
    normed_part = lax.dynamic_slice_in_dim(normed, column, width, 1)
    flat_expert = routes.reshape(-1)
    picks = (flat_expert[:, None] == jnp.arange(groups, dtype=jnp.int32)[None, :]).astype(jnp.int32)
    ranking = jnp.sum((jnp.cumsum(picks, axis=0) - 1) * picks, axis=1)
    target = flat_expert * capacity + ranking
    token_of = jnp.arange(length * chosen_count, dtype=jnp.int32) // chosen_count
    slot_token = jnp.zeros((groups * capacity,), jnp.int32).at[target].set(token_of + 1)
    filled = (slot_token > 0)[:, None]
    source_row = jnp.maximum(slot_token - 1, 0)
    nothing = jnp.zeros((), jnp.bfloat16)
    outgoing = jnp.where(filled, jnp.take(normed_part, source_row, axis=0), nothing).reshape(
        groups, capacity, width
    )
    arrived = lax.all_to_all(outgoing, "sp", split_axis=0, concat_axis=0, tiled=True)
    piece = lax.all_gather(arrived, "tp", axis=2, tiled=True)
    span = piece.shape[2]
    flat = piece.reshape(-1, span)
    gate_rows = w_gate[0]
    up_rows = w_up[0]
    gate = jnp.dot(flat, gate_rows, preferred_element_type=jnp.float32)
    upper = jnp.dot(flat, up_rows, preferred_element_type=jnp.float32)
    returned = finish(gate, upper, w_down).reshape(groups, capacity, width)
    landed = lax.all_to_all(returned, "sp", split_axis=0, concat_axis=0, tiled=True)
    flat_back = landed.reshape(groups * capacity, width)
    fetched = (
        jnp.take(flat_back, target, axis=0).astype(jnp.float32).reshape(length, chosen_count, width)
    )
    weighted = jnp.sum(fetched * route_weight[:, :, None], axis=1)
    return (own_part + weighted).astype(jnp.bfloat16)


def solution(mesh):
    return jax.shard_map(
        body,
        mesh=mesh,
        in_specs=(
            P("sp", "tp"),
            P("sp", "tp"),
            P("sp", "tp"),
            P(None, "tp"),
            P("sp"),
            P("tp", None),
            P("sp", None),
            P(),
            P("sp", None),
            P("sp", None),
            P("sp", None, "tp"),
            P("sp", None, "tp"),
            P("sp", "tp", None),
        ),
        out_specs=P("sp", "tp"),
        check_vma=False,
    )
```

profile of v0, /device:TPU:0, one launch (start us, length us, event | category | flops | bytes accessed | tf_op | source)
XLA Modules:
  0.0 246.0 jit_solution(10779795874960128418)
XLA Ops:
  6.5 0.0 copy-start
  6.5 0.0 copy-start.2
  6.5 0.0 all-reduce.2.cloned.1.call-start
  6.5 0.8 convert_element_type.53
  7.4 0.1 slice.35
  7.4 2.4 collective-permute-start
  9.8 1.0 convert_multiply_fusion
  10.9 4.6 %collective-permute-start.1 = (f32[2,256]{1,0:T(2,128)S(1)}, f32[2,256]{1,0:T(2,128)S(1)}, u32[]{:S(2)}, u32[]{:S(2)}) collective-permute-start(f32[2,256]{1,0:T(2,128)S(1)} %slice.50), channel_id=1, source_target_pairs={{0,4},{4,8},{8,12},{12,16},{16,20},{20,24},{24,28},{1,5},{5,9},{9,... | collective-permute-start | bytes 6152 | tf_op jit(solution)/shard_map/ppermute | solution.py:10
  15.4 0.8 copy.20
  16.3 0.7 broadcast_multiply_fusion
  17.0 0.8 fusion.37
  17.7 0.1 eq.34
  17.9 1.1 reduce-window.6
  19.0 0.0 collective-permute-done
  19.1 0.1 pad_maximum_fusion.1
  19.1 0.8 slice_compare_fusion.1
  19.9 0.0 collective-permute-done.1
  19.9 0.0 copy-done
  19.9 2.5 %convolution_convert_fusion = bf16[256,2048]{1,0:T(8,128)(2,1)} fusion(bf16[256,2048]{1,0:T(8,128)(2,1)S(1)} %copy-done, f32[2,256]{1,0:T(2,128)S(1)} %collective-permute-done.1, f32[256,256]{1,0:T(8,128)S(1)} %convert_multiply_fusion, bf16[256,256]{1,0:T(8,128)(2,1)} %param.13, f32[256]{0:T(256)S(1)} %bitcast.40, f32[256]{0:T(256)S(1)} %bitcast.39, ...), kind=kOutput, calls=%fused_computation.11 | convolution fusion | flops 269746176 | bytes 2496000 | tf_op jit(solution)/shard_map/dot_general | solution.py:55
  22.4 0.0 all-reduce.2.cloned.1.call-update
  22.4 0.0 all-gather.2.cloned.1.call-start
  22.4 0.2 slice_reduce_fusion
  22.7 0.1 reshape.103
  22.8 0.1 copy.24
  23.0 0.1 mul.110
  23.1 0.1 fusion.27
  23.2 2.4 scatter_custom_fusion
  25.7 0.1 broadcast_in_dim.68
  25.8 0.1 broadcast_in_dim.70
  25.9 0.8 dynamic-slice
  26.7 48.6 %all-reduce.2.cloned.1.call-done = bf16[256,2048]{1,0:T(8,128)(2,1)} async-done(((bf16[256,2048]{1,0:T(8,128)(2,1)}), bf16[256,2048]{1,0:T(8,128)(2,1)}) %all-reduce.2.cloned.1.call-update) | async-done | bytes 1048592 | tf_op jit(solution)/shard_map/psum | solution.py:56
  75.2 0.0 copy-done.2
  75.2 1.6 multiply_reduce_fusion
  76.9 0.0 copy-start.1
  76.9 1.4 copy-done.1
  78.3 0.1 multiply_convert_fusion.1
  78.4 2.7 %gather_fusion = bf16[768,512]{1,0:T(8,128)(2,1)S(1)} fusion(bf16[256,512]{1,0:T(8,128)(2,1)S(1)} %multiply_convert_fusion.1, s32[1024]{0:T(1024)S(1)} %pad_clamp_fusion.1), kind=kCustom, calls=%fused_computation | custom fusion | bytes 1575936 | tf_op jit(solution)/shard_map/jit(_take)/gather | solution.py:72
  81.1 0.3 select_select_fusion
  81.4 25.5 %all_to_all.10 = bf16[8,96,512]{2,1,0:T(8,128)(2,1)} all-to-all(bf16[8,96,512]{2,1,0:T(8,128)(2,1)S(1)} %select_select_fusion), channel_id=1, replica_groups=mesh['sp'=8,'tp'=4] {'sp'}, dimensions={0} | all-to-all | bytes 1572864 | tf_op jit(solution)/shard_map/all_to_all | solution.py:75
  106.8 0.0 all-gather.2.cloned.1.call-update
  106.8 0.0 reduce-scatter.2.cloned.1.call-start
  106.9 41.8 %all-gather.2.cloned.1.call-done = bf16[8,96,2048]{2,1,0:T(8,128)(2,1)} async-done(((bf16[8,96,512]{2,1,0:T(8,128)(2,1)}), bf16[8,96,2048]{2,1,0:T(8,128)(2,1)}) %all-gather.2.cloned.1.call-update) | async-done | bytes 3145744 | tf_op jit(solution)/shard_map/all_gather | solution.py:76
  148.7 0.0 copy-start.5
  148.7 6.3 %fusion.2 = f32[768,1024]{1,0:T(8,128)S(1)} fusion(bf16[768,2048]{1,0:T(8,128)(2,1)} %bitcast.41, bf16[1,2048,1024]{2,1,0:T(8,128)(2,1)} %param.24), kind=kOutput, calls=%fused_computation.5 | convolution fusion | flops 3221225472 | bytes 10485760 | tf_op jit(solution)/shard_map/dot_general | solution.py:82
  154.9 0.0 copy-done.5
  155.0 0.0 copy-done.7
  155.0 0.0 copy-start.6
  155.0 3.8 %multiply_convert_fusion = bf16[768,1024]{1,0:T(8,128)(2,1)S(1)} fusion(f32[768,1024]{1,0:T(8,128)S(1)} %fusion.2, bf16[768,2048]{1,0:T(8,128)(2,1)S(1)} %bitcast.42, bf16[1,2048,1024]{2,1,0:T(8,128)(2,1)S(1)} %copy-done.5), kind=kOutput, calls=%fused_computation.10 | convolution fusion | flops 3225944064 | bytes 12058624 | tf_op jit(solution)/shard_map/dot_general | solution.py:81
  158.8 0.0 copy-done.6
  158.8 4.8 %fusion.6 = bf16[768,2048]{1,0:T(8,128)(2,1)} fusion(bf16[768,1024]{1,0:T(8,128)(2,1)S(1)} %multiply_convert_fusion, bf16[1,1024,2048]{2,1,0:T(8,128)(2,1)S(1)} %copy-done.6), kind=kOutput, calls=%fused_computation.9 | convolution fusion | flops 3222798336 | bytes 8912896 | tf_op jit(solution)/shard_map/dot_general | solution.py:15
  163.6 0.0 reduce-scatter.2.cloned.1.call-update
  163.6 44.1 %reduce-scatter.2.cloned.1.call-done = bf16[768,512]{1,0:T(8,128)(2,1)} async-done(((bf16[768,2048]{1,0:T(8,128)(2,1)}), bf16[768,512]{1,0:T(8,128)(2,1)}) %reduce-scatter.2.cloned.1.call-update) | async-done | bytes 786448 | tf_op jit(solution)/shard_map/reduce_scatter | solution.py:16
  207.7 4.6 %all-to-all-start.1 = ((bf16[8,96,512]{2,1,0:T(8,128)(2,1)}), bf16[8,96,512]{2,1,0:T(8,128)(2,1)S(1)}, u32[]{:S(2)}, u32[]{:S(2)}) async-start(bf16[8,96,512]{2,1,0:T(8,128)(2,1)} %bitcast.34), calls=%async_computation.2 | async-start | bytes 1572864 | tf_op jit(solution)/shard_map/all_to_all | solution.py:84
  212.3 0.1 reduce_sum.32
  212.4 0.1 copy.22
  212.5 0.0 copy-done.3
  212.5 0.2 copy.23
  212.7 0.0 copy-done.4
  212.7 0.1 copy.25
  212.9 20.4 %all-to-all-done.1 = bf16[8,96,512]{2,1,0:T(8,128)(2,1)S(1)} async-done(((bf16[8,96,512]{2,1,0:T(8,128)(2,1)}), bf16[8,96,512]{2,1,0:T(8,128)(2,1)S(1)}, u32[]{:S(2)}, u32[]{:S(2)}) %all-to-all-start.1) | async-done | bytes 786464 | tf_op jit(solution)/shard_map/all_to_all | solution.py:84
  233.2 2.0 gather_fusion.1
  235.2 0.2 gather.15
  235.4 2.2 multiply_reduce_fusion.1
  237.6 1.8 add_convert_fusion
  (15 shorter events, 0.1 us)
Async XLA Ops:
  6.5 13.4 %copy-start = (bf16[256,2048]{1,0:T(8,128)(2,1)S(1)}, bf16[256,2048]{1,0:T(8,128)(2,1)}, u32[]{:S(2)}) copy-start(bf16[256,2048]{1,0:T(8,128)(2,1)} %param.18) | copy-start | bytes 3145732
  6.5 68.7 %copy-start.2 = (bf16[256,2048]{1,0:T(8,128)(2,1)S(1)}, bf16[256,2048]{1,0:T(8,128)(2,1)}, u32[]{:S(2)}) copy-start(bf16[256,2048]{1,0:T(8,128)(2,1)} %param.19) | copy-start | bytes 3145732
  6.5 68.7 %all-reduce.2.cloned.1.call-start = ((), (), s32[]{:S(2)}) async-start(), calls=%async_computation.3 | async-start | bytes 2097152 | tf_op jit(solution)/shard_map/psum | solution.py:56
  7.4 11.6 %collective-permute-start = (f32[2]{0:T(128)S(1)}, f32[2]{0:T(128)S(1)}, u32[]{:S(2)}, u32[]{:S(2)}) collective-permute-start(f32[2]{0:T(128)S(1)} %slice.35), channel_id=1, source_target_pairs={{0,4},{4,8},{8,12},{12,16},{16,20},{20,24},{24,28},{1,5},{5,9},{9,... | collective-permute-start | bytes 32 | tf_op jit(solution)/shard_map/ppermute | solution.py:10
  10.9 9.0 %collective-permute-start.1 = (f32[2,256]{1,0:T(2,128)S(1)}, f32[2,256]{1,0:T(2,128)S(1)}, u32[]{:S(2)}, u32[]{:S(2)}) collective-permute-start(f32[2,256]{1,0:T(2,128)S(1)} %slice.50), channel_id=1, source_target_pairs={{0,4},{4,8},{8,12},{12,16},{16,20},{20,24},{24,28},{1,5},{5,9},{9,... | collective-permute-start | bytes 6152 | tf_op jit(solution)/shard_map/ppermute | solution.py:10
  22.4 126.3 %all-gather.2.cloned.1.call-start = ((), (), s32[]{:S(2)}) async-start(), calls=%async_computation.4 | async-start | bytes 3932160 | tf_op jit(solution)/shard_map/all_gather | solution.py:76
  76.9 1.4 copy-start.1
  106.8 100.9 %reduce-scatter.2.cloned.1.call-start = ((), (), s32[]{:S(2)}) async-start(), calls=%async_computation.5 | async-start | bytes 3932160 | tf_op jit(solution)/shard_map/reduce_scatter | solution.py:16
  148.7 6.3 %copy-start.5 = (bf16[1,2048,1024]{2,1,0:T(8,128)(2,1)S(1)}, bf16[1,2048,1024]{2,1,0:T(8,128)(2,1)}, u32[]{:S(2)}) copy-start(bf16[1,2048,1024]{2,1,0:T(8,128)(2,1)} %param.23) | copy-start | bytes 12582916
  148.7 6.3 %copy-start.7 = (bf16[8,96,2048]{2,1,0:T(8,128)(2,1)S(1)}, bf16[8,96,2048]{2,1,0:T(8,128)(2,1)}, u32[]{:S(2)}) copy-start(bf16[8,96,2048]{2,1,0:T(8,128)(2,1)} %all-gather.2.cloned.1.call-done) | copy-start | bytes 9437188
  155.0 3.8 %copy-start.6 = (bf16[1,1024,2048]{2,1,0:T(8,128)(2,1)S(1)}, bf16[1,1024,2048]{2,1,0:T(8,128)(2,1)}, u32[]{:S(2)}) copy-start(bf16[1,1024,2048]{2,1,0:T(8,128)(2,1)} %param.25) | copy-start | bytes 12582916
  163.6 48.9 %copy-start.3 = (s32[256,2]{0,1:T(2,128)S(1)}, s32[256,2]{0,1:T(2,128)}, u32[]{:S(2)}) copy-start(s32[256,2]{0,1:T(2,128)} %param.21) | copy-start | bytes 6148
  163.6 49.1 %copy-start.4 = (f32[256,2]{0,1:T(2,128)S(1)}, f32[256,2]{0,1:T(2,128)}, u32[]{:S(2)}) copy-start(f32[256,2]{0,1:T(2,128)} %param.22) | copy-start | bytes 6148
  207.7 25.5 %all-to-all-start.1 = ((bf16[8,96,512]{2,1,0:T(8,128)(2,1)}), bf16[8,96,512]{2,1,0:T(8,128)(2,1)S(1)}, u32[]{:S(2)}, u32[]{:S(2)}) async-start(bf16[8,96,512]{2,1,0:T(8,128)(2,1)} %bitcast.34), calls=%async_computation.2 | async-start | bytes 1572864 | tf_op jit(solution)/shard_map/all_to_all | solution.py:84
Sparse Core Ops, SparseCore 0:
  22.5 52.6 all-reduce.1
  106.9 41.6 all-gather.1
  163.7 43.8 reduce-scatter.1
where the time goes:
time: 246 us
  waiting for transfers between devices  155 us (63%)
  blocking collectives  25.5 us (10%)
  matrix products  17.4 us (7%)
  between operations  13.4 us (5%)
  local copies, waits for them, and re-layouts  12.6 us (5%)
  starting transfers between devices  11.7 us (5%)
  other arithmetic  10.7 us (4%)
    psum x1, waiting for transfers between devices, body(): lax.psum(partial_value.astype(jnp.bfloat16), 'tp').astype(jnp.float32)  48.6 us
    reduce_scatter x1, waiting for transfers between devices, finish(): lax.psum_scatter(partial_value.astype(jnp.bfloat16), 'tp', scatter_dimens...  44.1 us
    all_gather x1, waiting for transfers between devices, body(): piece = lax.all_gather(arrived, 'tp', axis=2, tiled=True)  41.8 us
    all_to_all x1, blocking collectives, body(): lax.all_to_all(outgoing, 'sp', split_axis=0, concat_axis=0, tiled=True)  25.5 us
    all_to_all x1, waiting for transfers between devices, body(): lax.all_to_all(returned, 'sp', split_axis=0, concat_axis=0, tiled=True)  20.4 us
    ppermute x2, starting transfers between devices, passed_along(): lax.ppermute(value, axis, [(source, source + steps) for source in range(f...  6.97 us
    dot_general x1, matrix products, body(): upper = jnp.dot(flat, up_rows, preferred_element_type=jnp.float32)  6.28 us
  transfers between devices with their start and end apart: 6, of which 4 were waited for; matrix products, arithmetic and copies ran while one was open for 4% of the time, Pallas kernels for 0%

commit v1 on v0

v1 whole, which is shorter than its diff:
```python
import functools

import jax
import jax.numpy as jnp
from jax import lax
from jax.experimental import pallas as pl
from jax.experimental.pallas import tpu as pltpu
from jax.sharding import PartitionSpec as P

F32 = jnp.float32
BF16 = jnp.bfloat16
MESH = pl.DeviceIdType.MESH
GROUP = 2


def xor(value, mask, count):
    out, bit = value, 1
    while bit < count:
        if isinstance(mask, int):
            if mask & bit:
                out = out + bit * (1 - 2 * lax.rem(lax.div(value, bit), 2))
        else:
            ours = lax.rem(lax.div(value, bit), 2)
            other = lax.rem(lax.div(mask, bit), 2)
            out = out + bit * other * (1 - 2 * ours)
        bit *= 2
    return out


def kernel(
    n_sp, n_tp, cap,
    outer, inner, vals, taps, doc, routes_c, routes_r, rw, gain,
    mix_hbm, stream_hbm, wg_hbm, wu_hbm, wd_hbm,
    out,
    mix, own, wg, wu, wd, rim_out, rim_in, prod_pad, doc_pad,
    bpart, brecv, hidden, obuf, xbuf, pbuf, r1, act, ret, back, acc,
    local_sem, rim_s, rim_r, br_s, br_r, z_s, z_r, ag_s, ag_r, rs_s, rs_r, bk_s, bk_r,
):
    s, p = lax.axis_index("sp"), lax.axis_index("tp")
    length, channels = outer.shape
    width = own.shape[1]
    features = mix.shape[1]
    hidden_units = wg.shape[1]
    x_side = 1
    while x_side * x_side < n_tp:
        x_side *= 2
    x_set = list(range(x_side))
    y_set = [k * x_side for k in range(n_tp // x_side)]

    def at(index):
        return pl.multiple_of(index * width, width)

    loads = [
        pltpu.make_async_copy(mix_hbm, mix, local_sem.at[0]),
        pltpu.make_async_copy(stream_hbm.at[:, pl.ds(at(p), width)], own, local_sem.at[1]),
        pltpu.make_async_copy(wg_hbm.at[0], wg, local_sem.at[2]),
        pltpu.make_async_copy(wu_hbm.at[0], wu, local_sem.at[3]),
        pltpu.make_async_copy(wd_hbm.at[0], wd, local_sem.at[4]),
    ]
    for load in loads:
        load.start()

    barrier = pltpu.get_barrier_semaphore()
    for d in range(1, n_sp):
        pl.semaphore_signal(barrier, inc=1, device_id={"sp": xor(s, d, n_sp)}, device_id_type=MESH)
    for r in range(1, n_tp):
        pl.semaphore_signal(barrier, inc=1, device_id={"tp": xor(p, r, n_tp)}, device_id_type=MESH)
    product = inner[...].astype(F32) * vals[...].astype(F32)
    prod_pad[8:, :] = product
    docs = jnp.broadcast_to(doc[...], (length, channels))
    doc_pad[8:, :] = docs
    rim_out[:8, :] = product[length - 8 :]
    rim_out[8:, :] = docs[length - 8 :]
    pl.semaphore_wait(barrier, n_sp - 1 + n_tp - 1)

    sends = []

    def send(src, dst, s_sem, r_sem, **device):
        copy = pltpu.make_async_remote_copy(
            src_ref=src, dst_ref=dst, send_sem=s_sem, recv_sem=r_sem,
            device_id=device, device_id_type=MESH,
        )
        copy.start()
        sends.append(copy)
        return copy

    rim = send(rim_out, rim_in, rim_s, rim_r, sp=lax.rem(s + 1, n_sp))

    row = lax.broadcasted_iota(jnp.int32, (length, length), 0)
    col = lax.broadcasted_iota(jnp.int32, (length, length), 1)
    expert_r = lax.broadcasted_iota(jnp.int32, (max(n_sp, 16), length), 0)
    in_r = ((routes_r[0:1, :] == expert_r) | (routes_r[1:2, :] == expert_r)).astype(F32)
    rank_r = jnp.dot(in_r.astype(BF16), (row < col).astype(F32).astype(BF16), preferred_element_type=F32)
    expert_c = lax.broadcasted_iota(jnp.int32, (length, 128), 1)
    in_c = ((routes_c[:, 0:1] == expert_c) | (routes_c[:, 1:2] == expert_c)).astype(F32)
    rank_c = jnp.dot((row > col).astype(F32).astype(BF16), in_c.astype(BF16), preferred_element_type=F32)
    rank_r = jnp.where(in_r > 0, rank_r, -1.0)
    rank_c = jnp.where(in_c > 0, rank_c, -1.0)

    loads[0].wait()
    rim.wait_recv()
    prod_pad[:8, :] = rim_in[:8, :]
    doc_pad[:8, :] = jnp.where(s > 0, rim_in[8:, :], -1.0)
    kernel_taps = taps[...].astype(F32)
    conv = kernel_taps[2:3] * product
    for step in (1, 2):
        same = doc_pad[pl.ds(8 - step, length), :] == docs
        conv = conv + kernel_taps[2 - step : 3 - step] * jnp.where(same, prod_pad[pl.ds(8 - step, length), :], 0.0)
    gated = (outer[...].astype(F32) * conv).astype(BF16)
    for r in list(range(n_tp - 1, 0, -1)) + [0]:
        q = xor(p, r, n_tp)
        bpart[r] = jnp.dot(gated, mix[:, pl.ds(at(q), width)], preferred_element_type=F32).astype(BF16)
        if r:
            send(bpart.at[r], brecv.at[r], br_s.at[r], br_r.at[r], tp=q)
    loads[1].wait()
    total = bpart[0].astype(F32)
    for r in range(1, n_tp):
        pltpu.make_async_copy(brecv.at[r], brecv.at[r], br_r.at[r]).wait()
        total = total + brecv[r].astype(F32)
    total = total + own[...].astype(F32)
    hidden[...] = total
    scaled = (total * gain[pl.ds(p, 1), :]).astype(BF16)

    slot_r = lax.broadcasted_iota(jnp.int32, (cap, length), 0).astype(F32)
    for d in list(range(n_sp)):
        e = xor(s, d, n_sp)
        line = jnp.sum(jnp.where(expert_r == e, rank_r, 0.0), axis=0, keepdims=True)
        pick = (line == slot_r).astype(F32).astype(BF16)
        rows = jnp.dot(pick, scaled, preferred_element_type=F32).astype(BF16)
        if d == 0:
            xbuf[0, 0] = rows
        else:
            obuf[d] = rows
            send(obuf.at[d], xbuf.at[0, d], z_s.at[d], z_r.at[d], sp=e)

    def arrived(ref, sem):
        pltpu.make_async_copy(ref, ref, sem).wait()

    def axes(d):
        return (x_set, y_set) if d % 2 == 0 else (y_set, x_set)

    def gather_first(d):
        first, _ = axes(d)
        if d:
            arrived(xbuf.at[0, d], z_r.at[d])
        for f in first[1:]:
            send(xbuf.at[0, d], xbuf.at[f, d], ag_s.at[d, f], ag_r.at[d, f], tp=xor(p, f, n_tp))

    def gather_second(d):
        first, second = axes(d)
        for f in first:
            if f:
                arrived(xbuf.at[f, d], ag_r.at[d, f])
            for g in second[1:]:
                send(
                    xbuf.at[f, d], xbuf.at[f + g, d], ag_s.at[d, f + g], ag_r.at[d, f + g],
                    tp=xor(p, g, n_tp),
                )

    tile = min(256, hidden_units)

    def expert(step):
        low = step * GROUP
        for d in range(low, low + GROUP):
            first, second = axes(d)
            for f in first:
                for g in second[1:]:
                    arrived(xbuf.at[f + g, d], ag_r.at[d, f + g])
        square = jnp.zeros((GROUP * cap, 1), F32)
        for r in range(n_tp):
            inverse = 1.0 / gain[pl.ds(xor(p, r, n_tp), 1), :]
            plain = xbuf[r, low : low + GROUP].reshape(GROUP * cap, width).astype(F32) * inverse
            square = square + jnp.sum(plain * plain, axis=1, keepdims=True)
        scale = lax.rsqrt(square / features + 1e-06)

        def up_tile(j, _):
            lanes = pl.ds(pl.multiple_of(j * tile, tile), tile)
            gate = jnp.zeros((GROUP * cap, tile), F32)
            upper = jnp.zeros((GROUP * cap, tile), F32)
            for r in range(n_tp):
                lhs = xbuf[r, low : low + GROUP].reshape(GROUP * cap, width)
                deep = pl.ds(at(xor(p, r, n_tp)), width)
                gate = gate + jnp.dot(lhs, wg[deep, lanes], preferred_element_type=F32)
                upper = upper + jnp.dot(lhs, wu[deep, lanes], preferred_element_type=F32)
            gate, upper = gate * scale, upper * scale
            act[:, lanes] = (gate / (1.0 + jnp.exp(-gate)) * upper).astype(BF16)
            return 0

        lax.fori_loop(0, hidden_units // tile, up_tile, 0)

        def down_tile(r, _):
            lanes = pl.ds(at(xor(p, r, n_tp)), width)
            part = jnp.dot(act[...], wd[:, lanes], preferred_element_type=F32).astype(BF16)
            pbuf[r, low : low + GROUP] = part.reshape(GROUP, cap, width)
            return 0

        lax.fori_loop(0, n_tp, down_tile, 0)
        for d in range(low, low + GROUP):
            first, second = axes(d)
            for f in first[1:]:
                for g in second[::-1]:
                    send(
                        pbuf.at[f + g, d], r1.at[f + g, d], rs_s.at[d, f + g], rs_r.at[d, f + g],
                        tp=xor(p, f, n_tp),
                    )

    def scatter_second(d):
        first, second = axes(d)
        for g in second[1:]:
            part = pbuf[g, d].astype(F32)
            for f in first[1:]:
                arrived(r1.at[f + g, d], rs_r.at[d, f + g])
                part = part + r1[f + g, d].astype(F32)
            pbuf[g, d] = part.astype(BF16)
            send(pbuf.at[g, d], r1.at[g, d], rs_s.at[d, g], rs_r.at[d, g], tp=xor(p, g, n_tp))

    def give_back(d):
        first, second = axes(d)
        part = pbuf[0, d].astype(F32)
        for k in first[1:] + second[1:]:
            arrived(r1.at[k, d], rs_r.at[d, k])
            part = part + r1[k, d].astype(F32)
        if d == 0:
            back[0] = part.astype(BF16)
        else:
            ret[d] = part.astype(BF16)
            send(ret.at[d], back.at[d], bk_s.at[d], bk_r.at[d], sp=xor(s, d, n_sp))

    slot_c = lax.broadcasted_iota(jnp.int32, (length, cap), 1).astype(F32)
    acc[...] = hidden[...]

    def combine(d):
        e = xor(s, d, n_sp)
        if d:
            arrived(back.at[d], bk_r.at[d])
        line = jnp.sum(jnp.where(expert_c == e, rank_c, 0.0), axis=1, keepdims=True)
        pick = (line == slot_c).astype(F32).astype(BF16)
        fetched = jnp.dot(pick, back[d], preferred_element_type=F32)
        weight = jnp.where(routes_c[:, 0:1] == e, rw[:, 0:1], 0.0) + jnp.where(routes_c[:, 1:2] == e, rw[:, 1:2], 0.0)
        acc[...] = acc[...] + fetched * weight

    steps = n_sp // GROUP
    stages = (gather_first, gather_second, expert, scatter_second, give_back, combine)
    for now in range(steps + len(stages) - 1):
        for behind, stage in enumerate(stages):
            step = now - behind
            if 0 <= step < steps:
                if stage is expert:
                    if step == 0:
                        for load in loads[2:]:
                            load.wait()
                    expert(step)
                else:
                    for d in range(step * GROUP, (step + 1) * GROUP):
                        stage(d)
    out[...] = acc[...].astype(out.dtype)
    for copy in sends:
        copy.wait_send()


def body(
    outer_gate, inner_gate, values, conv_taps, document, mix_proj, stream, norm_gain,
    routes, route_weight, w_gate, w_up, w_down,
):
    length, features = stream.shape
    channels = outer_gate.shape[1]
    n_sp, n_tp = lax.axis_size("sp"), lax.axis_size("tp")
    width = features // n_tp
    units = w_gate.shape[2]
    cap = -(-(3 * length // n_sp) // 16) * 16
    vmem, anywhere = pl.BlockSpec(memory_space=pltpu.VMEM), pl.BlockSpec(memory_space=pl.ANY)
    block = (n_sp, cap, width)
    dma = pltpu.SemaphoreType.DMA
    return pl.pallas_call(
        functools.partial(kernel, n_sp, n_tp, cap),
        out_shape=jax.ShapeDtypeStruct((length, width), BF16),
        in_specs=[vmem] * 9 + [anywhere] * 5,
        out_specs=vmem,
        scratch_shapes=[
            pltpu.VMEM((channels, features), BF16),
            pltpu.VMEM((length, width), BF16),
            pltpu.VMEM((features, units), BF16),
            pltpu.VMEM((features, units), BF16),
            pltpu.VMEM((units, features), BF16),
            pltpu.VMEM((16, channels), F32),
            pltpu.VMEM((16, channels), F32),
            pltpu.VMEM((length + 8, channels), F32),
            pltpu.VMEM((length + 8, channels), F32),
            pltpu.VMEM((n_tp, length, width), BF16),
            pltpu.VMEM((n_tp, length, width), BF16),
            pltpu.VMEM((length, width), F32),
            pltpu.VMEM(block, BF16),
            pltpu.VMEM((n_tp,) + block, BF16),
            pltpu.VMEM((n_tp,) + block, BF16),
            pltpu.VMEM((n_tp,) + block, BF16),
            pltpu.VMEM((GROUP * cap, units), BF16),
            pltpu.VMEM(block, BF16),
            pltpu.VMEM(block, BF16),
            pltpu.VMEM((length, width), F32),
            dma((5,)), dma, dma, dma((n_tp,)), dma((n_tp,)), dma((n_sp,)), dma((n_sp,)),
            dma((n_sp, n_tp)), dma((n_sp, n_tp)), dma((n_sp, n_tp)), dma((n_sp, n_tp)),
            dma((n_sp,)), dma((n_sp,)),
        ],
        compiler_params=pltpu.CompilerParams(
            collective_id=0, has_side_effects=True, vmem_limit_bytes=56 << 20
        ),
    )(
        outer_gate, inner_gate, values, conv_taps, document.astype(F32).reshape(-1, 1),
        routes, routes.T, route_weight, norm_gain.reshape(n_tp, width),
        mix_proj, stream, w_gate, w_up, w_down,
    )


def solution(mesh):
    return jax.shard_map(
        body,
        mesh=mesh,
        in_specs=(
            P("sp", "tp"),
            P("sp", "tp"),
            P("sp", "tp"),
            P(None, "tp"),
            P("sp"),
            P("tp", None),
            P("sp", None),
            P(),
            P("sp", None),
            P("sp", None),
            P("sp", None, "tp"),
            P("sp", None, "tp"),
            P("sp", "tp", None),
        ),
        out_specs=P("sp", "tp"),
        check_vma=False,
    )
```

time: 246 us -> 104 us (0.42)
  waiting for transfers between devices: 155 us -> 0 us
  Pallas kernels: 0 us -> 95.3 us
  blocking collectives: 25.5 us -> 0 us
  matrix products: 17.4 us -> 0 us
  between operations: 13.4 us -> 0.01 us
  starting transfers between devices: 11.7 us -> 0 us
  other arithmetic: 10.7 us -> 0.68 us
  local copies, waits for them, and re-layouts: 12.6 us -> 6.71 us
    pallas_call x0 -> x1, Pallas kernels: none -> 95.3 us  [body(): pl.pallas_call(functools.partial(kernel, n_sp, n_tp, cap), out_shape=jax....]
    psum x1 -> x0, waiting for transfers between devices: 48.6 us -> none  [body(): lax.psum(partial_value.astype(jnp.bfloat16), 'tp').astype(jnp.float32)]
    reduce_scatter x1 -> x0, waiting for transfers between devices: 44.1 us -> none  [finish(): lax.psum_scatter(partial_value.astype(jnp.bfloat16), 'tp', scatter_dimens...]
    all_gather x1 -> x0, waiting for transfers between devices: 41.8 us -> none  [body(): piece = lax.all_gather(arrived, 'tp', axis=2, tiled=True)]
    all_to_all x1 -> x0, blocking collectives: 25.5 us -> none  [body(): lax.all_to_all(outgoing, 'sp', split_axis=0, concat_axis=0, tiled=True)]
    all_to_all x1 -> x0, waiting for transfers between devices: 20.4 us -> none  [body(): lax.all_to_all(returned, 'sp', split_axis=0, concat_axis=0, tiled=True)]
    dot_general x4 -> x0, matrix products: 17.4 us -> none  [the longest x1 6.28 us: body(): upper = jnp.dot(flat, up_rows, preferred_element_type=jnp.float32)]
    ppermute x2 -> x0, starting transfers between devices: 6.97 us -> none  [passed_along(): lax.ppermute(value, axis, [(source, source + steps) for source in range(f...]
  transfers between devices with their start and end apart: 6 -> 0, of which waited for: 4 -> 0; matrix products, arithmetic and copies ran while one was open for 4% -> 0% of each run, Pallas kernels for 0% -> 0%
where the time goes in v1:
time: 104 us; the launch traced here: 103 us
  Pallas kernels  95.3 us (92%)
  local copies, waits for them, and re-layouts  6.71 us (6%)
    pallas_call x1, Pallas kernels, body(): pl.pallas_call(functools.partial(kernel, n_sp, n_tp, cap), out_shape=jax....  95.3 us
    unnamed x3, local copies, waits for them, and re-layouts  4.62 us

profile of v1, /device:TPU:0, one launch (start us, length us, event | category | flops | bytes accessed | tf_op | source)
XLA Modules:
  0.0 102.7 jit_solution(8667715386031346197)
XLA Ops:
  0.0 0.7 convert_element_type.3
  0.7 1.3 %reshape.7.gain = f32[4,512]{1,0:T(4,128)} reshape(f32[2048]{0:T(1024)} %param.20) | data formatting | bytes 16384 | tf_op jit(solution)/shard_map/reshape | solution.py:309
  2.0 0.8 copy.16.doc
  2.8 1.5 %copy.18.rw = f32[256,2]{1,0:T(8,128)} copy(f32[256,2]{0,1:T(2,128)} %param.22) | data formatting | bytes 4096 | tf_op args[9]
  4.2 1.5 %copy.17.routes_c = s32[256,2]{1,0:T(8,128)} copy(s32[256,2]{0,1:T(2,128)} %param.21) | data formatting | bytes 4096 | tf_op args[8]
  5.7 95.3 %shard_map.127 = bf16[256,512]{1,0:T(8,128)(2,1)} custom-call(bf16[256,256]{1,0:T(8,128)(2,1)} %outer.1, bf16[256,256]{1,0:T(8,128)(2,1)} %inner.1, bf16[256,256]{1,0:T(8,128)(2,1)} %vals.1, bf16[3,256]{1,0:T(4,128)(2,1)} %taps.1, f32[256,1]{1,0:T(8,128)} %copy.16.doc, s32[256,2]{1,0:T(8,128)} %copy.17.routes_c, s32[2,256]{1,0:T(2,128)} %bitcast.2, ...), custom_call_target="tpu_custom_call" | custom-call | tf_op jit(solution)/shard_map/pallas_call | solution.py:274
  101.1 1.7 %copy.20 = bf16[256,512]{1,0:T(8,128)(2,1)} copy(bf16[256,512]{1,0:T(8,128)(2,1)} %shard_map.127) | data formatting | bytes 524288

commit v2 on v1

--- a/solution.py
+++ b/solution.py
@@ -10,7 +10,8 @@
 F32 = jnp.float32
 BF16 = jnp.bfloat16
 MESH = pl.DeviceIdType.MESH
-GROUP = 2
+GROUP = 1
+HEAD = 16
 
 
 def xor(value, mask, count):
@@ -29,12 +30,12 @@
 
 def kernel(
     n_sp, n_tp, cap,
-    outer, inner, vals, taps, doc, routes_c, routes_r, rw, gain,
-    mix_hbm, stream_hbm, wg_hbm, wu_hbm, wd_hbm,
+    taps, doc_r, routes_r, rw_r, gain,
+    outer_hbm, inner_hbm, vals_hbm, mix_hbm, stream_hbm, wg_hbm, wu_hbm, wd_hbm,
     out,
-    mix, own, wg, wu, wd, rim_out, rim_in, prod_pad, doc_pad,
-    bpart, brecv, hidden, obuf, xbuf, pbuf, r1, act, ret, back, acc,
-    local_sem, rim_s, rim_r, br_s, br_r, z_s, z_r, ag_s, ag_r, rs_s, rs_r, bk_s, bk_r,
+    outer, inner, vals, mix, own, wg, wu, wd, rim_out, rim_in, prod_pad, doc_pad,
+    bpart, brecv, head, hidden, obuf, xbuf, pbuf, r1, act, ret, back, acc,
+    local_sem, rim_s, rim_r, br_s, br_r, hd_s, hd_r, z_s, z_r, ag_s, ag_r, rs_s, rs_r, bk_s, bk_r,
 ):
     s, p = lax.axis_index("sp"), lax.axis_index("tp")
     length, channels = outer.shape
@@ -51,11 +52,16 @@
         return pl.multiple_of(index * width, width)
 
     loads = [
-        pltpu.make_async_copy(mix_hbm, mix, local_sem.at[0]),
-        pltpu.make_async_copy(stream_hbm.at[:, pl.ds(at(p), width)], own, local_sem.at[1]),
-        pltpu.make_async_copy(wg_hbm.at[0], wg, local_sem.at[2]),
-        pltpu.make_async_copy(wu_hbm.at[0], wu, local_sem.at[3]),
-        pltpu.make_async_copy(wd_hbm.at[0], wd, local_sem.at[4]),
+        pltpu.make_async_copy(inner_hbm, inner, local_sem.at[0]),
+        pltpu.make_async_copy(vals_hbm, vals, local_sem.at[1]),
+        pltpu.make_async_copy(outer_hbm, outer, local_sem.at[2]),
+        pltpu.make_async_copy(mix_hbm, mix, local_sem.at[3]),
+        pltpu.make_async_copy(stream_hbm.at[:, pl.ds(at(p), width)], own, local_sem.at[4]),
+    ]
+    weight_loads = [
+        pltpu.make_async_copy(wg_hbm.at[0], wg, local_sem.at[5]),
+        pltpu.make_async_copy(wu_hbm.at[0], wu, local_sem.at[6]),
+        pltpu.make_async_copy(wd_hbm.at[0], wd, local_sem.at[7]),
     ]
     for load in loads:
         load.start()
@@ -65,12 +71,40 @@
         pl.semaphore_signal(barrier, inc=1, device_id={"sp": xor(s, d, n_sp)}, device_id_type=MESH)
     for r in range(1, n_tp):
         pl.semaphore_signal(barrier, inc=1, device_id={"tp": xor(p, r, n_tp)}, device_id_type=MESH)
+    lines = [routes_r[...].astype(F32), rw_r[...], doc_r[...].astype(F32)]
+    table = jnp.concatenate(lines + [jnp.zeros((3, length), F32)], axis=0)
+    table = jnp.concatenate([table] * 16, axis=0).T
+    chosen = [table[:, 0:1], table[:, 1:2]]
+    chosen_weight = [table[:, 2:3], table[:, 3:4]]
+    docs = jnp.broadcast_to(table[:, 4:5], (length, channels))
+    loads[0].wait()
+    loads[1].wait()
     product = inner[...].astype(F32) * vals[...].astype(F32)
     prod_pad[8:, :] = product
-    docs = jnp.broadcast_to(doc[...], (length, channels))
     doc_pad[8:, :] = docs
     rim_out[:8, :] = product[length - 8 :]
     rim_out[8:, :] = docs[length - 8 :]
+    kernel_taps = taps[...].astype(F32)
+
+    def gated(count):
+        conv = kernel_taps[2:3] * product[:count]
+        for step in (1, 2):
+            same = doc_pad[pl.ds(8 - step, count), :] == docs[:count]
+            before = prod_pad[pl.ds(8 - step, count), :]
+            conv = conv + kernel_taps[2 - step : 3 - step] * jnp.where(same, before, 0.0)
+        return (outer[:count, :].astype(F32) * conv).astype(BF16)
+
+    def branch_part(rows, r):
+        lanes = pl.ds(at(xor(p, r, n_tp)), width)
+        return jnp.dot(rows, mix[:, lanes], preferred_element_type=F32).astype(BF16)
+
+    prod_pad[:8, :] = jnp.zeros((8, channels), F32)
+    doc_pad[:8, :] = jnp.full((8, channels), -1.0, F32)
+    loads[2].wait()
+    loads[3].wait()
+    rows = gated(length)
+    for r in range(n_tp):
+        bpart[r] = branch_part(rows, r)
     pl.semaphore_wait(barrier, n_sp - 1 + n_tp - 1)
 
     sends = []
@@ -85,45 +119,46 @@
         return copy
 
     rim = send(rim_out, rim_in, rim_s, rim_r, sp=lax.rem(s + 1, n_sp))
+    for r in range(n_tp - 1, 0, -1):
+        rest = pl.ds(HEAD, length - HEAD)
+        send(bpart.at[r, rest], brecv.at[r, rest], br_s.at[r], br_r.at[r], tp=xor(p, r, n_tp))
+    for load in weight_loads:
+        load.start()
 
     row = lax.broadcasted_iota(jnp.int32, (length, length), 0)
     col = lax.broadcasted_iota(jnp.int32, (length, length), 1)
     expert_r = lax.broadcasted_iota(jnp.int32, (max(n_sp, 16), length), 0)
     in_r = ((routes_r[0:1, :] == expert_r) | (routes_r[1:2, :] == expert_r)).astype(F32)
     rank_r = jnp.dot(in_r.astype(BF16), (row < col).astype(F32).astype(BF16), preferred_element_type=F32)
-    expert_c = lax.broadcasted_iota(jnp.int32, (length, 128), 1)
-    in_c = ((routes_c[:, 0:1] == expert_c) | (routes_c[:, 1:2] == expert_c)).astype(F32)
+    expert_c = lax.broadcasted_iota(jnp.int32, (length, 128), 1).astype(F32)
+    in_c = ((chosen[0] == expert_c) | (chosen[1] == expert_c)).astype(F32)
     rank_c = jnp.dot((row > col).astype(F32).astype(BF16), in_c.astype(BF16), preferred_element_type=F32)
     rank_r = jnp.where(in_r > 0, rank_r, -1.0)
     rank_c = jnp.where(in_c > 0, rank_c, -1.0)
 
-    loads[0].wait()
     rim.wait_recv()
     prod_pad[:8, :] = rim_in[:8, :]
     doc_pad[:8, :] = jnp.where(s > 0, rim_in[8:, :], -1.0)
-    kernel_taps = taps[...].astype(F32)
-    conv = kernel_taps[2:3] * product
-    for step in (1, 2):
-        same = doc_pad[pl.ds(8 - step, length), :] == docs
-        conv = conv + kernel_taps[2 - step : 3 - step] * jnp.where(same, prod_pad[pl.ds(8 - step, length), :], 0.0)
-    gated = (outer[...].astype(F32) * conv).astype(BF16)
-    for r in list(range(n_tp - 1, 0, -1)) + [0]:
-        q = xor(p, r, n_tp)
-        bpart[r] = jnp.dot(gated, mix[:, pl.ds(at(q), width)], preferred_element_type=F32).astype(BF16)
+    rows = gated(HEAD)
+    for r in range(n_tp - 1, -1, -1):
+        head[r] = branch_part(rows, r)
         if r:
-            send(bpart.at[r], brecv.at[r], br_s.at[r], br_r.at[r], tp=q)
-    loads[1].wait()
+            send(head.at[r], brecv.at[r, pl.ds(0, HEAD)], hd_s.at[r], hd_r.at[r], tp=xor(p, r, n_tp))
+    bpart[0, :HEAD] = head[0]
+    loads[4].wait()
     total = bpart[0].astype(F32)
     for r in range(1, n_tp):
-        pltpu.make_async_copy(brecv.at[r], brecv.at[r], br_r.at[r]).wait()
+        for rows, sem in ((pl.ds(HEAD, length - HEAD), br_r), (pl.ds(0, HEAD), hd_r)):
+            pltpu.make_async_copy(brecv.at[r, rows], brecv.at[r, rows], sem.at[r]).wait()
         total = total + brecv[r].astype(F32)
     total = total + own[...].astype(F32)
     hidden[...] = total
-    scaled = (total * gain[pl.ds(p, 1), :]).astype(BF16)
+    scaled = (total * gain[:, pl.ds(at(p), width)]).astype(BF16)
 
     slot_r = lax.broadcasted_iota(jnp.int32, (cap, length), 0).astype(F32)
-    for d in list(range(n_sp)):
-        e = xor(s, d, n_sp)
+    turn = [0, 2, 4, 6, 3, 5, 7, 1] + list(range(8, n_sp))
+    for d in range(n_sp):
+        e = xor(s, turn[d], n_sp)
         line = jnp.sum(jnp.where(expert_r == e, rank_r, 0.0), axis=0, keepdims=True)
         pick = (line == slot_r).astype(F32).astype(BF16)
         rows = jnp.dot(pick, scaled, preferred_element_type=F32).astype(BF16)
@@ -159,8 +194,7 @@
 
     tile = min(256, hidden_units)
 
-    def expert(step):
-        low = step * GROUP
+    def expert_up(low):
         for d in range(low, low + GROUP):
             first, second = axes(d)
             for f in first:
@@ -168,7 +202,7 @@
                     arrived(xbuf.at[f + g, d], ag_r.at[d, f + g])
         square = jnp.zeros((GROUP * cap, 1), F32)
         for r in range(n_tp):
-            inverse = 1.0 / gain[pl.ds(xor(p, r, n_tp), 1), :]
+            inverse = 1.0 / gain[:, pl.ds(at(xor(p, r, n_tp)), width)]
             plain = xbuf[r, low : low + GROUP].reshape(GROUP * cap, width).astype(F32) * inverse
             square = square + jnp.sum(plain * plain, axis=1, keepdims=True)
         scale = lax.rsqrt(square / features + 1e-06)
@@ -188,21 +222,19 @@
 
         lax.fori_loop(0, hidden_units // tile, up_tile, 0)
 
-        def down_tile(r, _):
+    def expert_down(low):
+        for r in range(n_tp - 1, -1, -1):
             lanes = pl.ds(at(xor(p, r, n_tp)), width)
             part = jnp.dot(act[...], wd[:, lanes], preferred_element_type=F32).astype(BF16)
             pbuf[r, low : low + GROUP] = part.reshape(GROUP, cap, width)
-            return 0
-
-        lax.fori_loop(0, n_tp, down_tile, 0)
-        for d in range(low, low + GROUP):
-            first, second = axes(d)
-            for f in first[1:]:
-                for g in second[::-1]:
-                    send(
-                        pbuf.at[f + g, d], r1.at[f + g, d], rs_s.at[d, f + g], rs_r.at[d, f + g],
-                        tp=xor(p, f, n_tp),
-                    )
+            for d in range(low, low + GROUP):
+                first, second = axes(d)
+                for f in first[1:]:
+                    if r - f in second:
+                        send(
+                            pbuf.at[r, d], r1.at[r, d], rs_s.at[d, r], rs_r.at[d, r],
+                            tp=xor(p, f, n_tp),
+                        )
 
     def scatter_second(d):
         first, second = axes(d)
@@ -224,35 +256,49 @@
             back[0] = part.astype(BF16)
         else:
             ret[d] = part.astype(BF16)
-            send(ret.at[d], back.at[d], bk_s.at[d], bk_r.at[d], sp=xor(s, d, n_sp))
+            send(ret.at[d], back.at[d], bk_s.at[d], bk_r.at[d], sp=xor(s, turn[d], n_sp))
 
     slot_c = lax.broadcasted_iota(jnp.int32, (length, cap), 1).astype(F32)
     acc[...] = hidden[...]
 
     def combine(d):
-        e = xor(s, d, n_sp)
+        e = xor(s, turn[d], n_sp)
         if d:
             arrived(back.at[d], bk_r.at[d])
-        line = jnp.sum(jnp.where(expert_c == e, rank_c, 0.0), axis=1, keepdims=True)
+        line = jnp.sum(jnp.where(expert_c == e.astype(F32), rank_c, 0.0), axis=1, keepdims=True)
         pick = (line == slot_c).astype(F32).astype(BF16)
         fetched = jnp.dot(pick, back[d], preferred_element_type=F32)
-        weight = jnp.where(routes_c[:, 0:1] == e, rw[:, 0:1], 0.0) + jnp.where(routes_c[:, 1:2] == e, rw[:, 1:2], 0.0)
+        weight = sum(jnp.where(c == e.astype(F32), w, 0.0) for c, w in zip(chosen, chosen_weight))
         acc[...] = acc[...] + fetched * weight
 
-    steps = n_sp // GROUP
-    stages = (gather_first, gather_second, expert, scatter_second, give_back, combine)
-    for now in range(steps + len(stages) - 1):
-        for behind, stage in enumerate(stages):
-            step = now - behind
-            if 0 <= step < steps:
-                if stage is expert:
-                    if step == 0:
-                        for load in loads[2:]:
-                            load.wait()
-                    expert(step)
+    def run(stage, *steps):
+        for step in steps:
+            if 0 <= step < count:
+                low = step * GROUP
+                if stage in (expert_up, expert_down):
+                    stage(low)
                 else:
-                    for d in range(step * GROUP, (step + 1) * GROUP):
+                    for d in range(low, low + GROUP):
                         stage(d)
+
+    count = n_sp // GROUP
+    run(gather_first, 0)
+    run(gather_first, 1)
+    run(gather_second, 0)
+    run(gather_first, 2)
+    run(gather_second, 1)
+    run(gather_first, 3)
+    run(gather_second, 2)
+    for load in weight_loads:
+        load.wait()
+    for step in range(count + 8):
+        run(expert_up, step + 0)
+        run(gather_first, step + 4)
+        run(gather_second, step + 3)
+        run(expert_down, step + 0)
+        run(scatter_second, step - 2)
+        run(give_back, step - 4)
+        run(combine, step - 6)
     out[...] = acc[...].astype(out.dtype)
     for copy in sends:
         copy.wait_send()
@@ -274,9 +320,12 @@
     return pl.pallas_call(
         functools.partial(kernel, n_sp, n_tp, cap),
         out_shape=jax.ShapeDtypeStruct((length, width), BF16),
-        in_specs=[vmem] * 9 + [anywhere] * 5,
+        in_specs=[vmem] * 5 + [anywhere] * 8,
         out_specs=vmem,
         scratch_shapes=[
+            pltpu.VMEM((length, channels), BF16),
+            pltpu.VMEM((length, channels), BF16),
+            pltpu.VMEM((length, channels), BF16),
             pltpu.VMEM((channels, features), BF16),
             pltpu.VMEM((length, width), BF16),
             pltpu.VMEM((features, units), BF16),
@@ -288,6 +337,7 @@
             pltpu.VMEM((length + 8, channels), F32),
             pltpu.VMEM((n_tp, length, width), BF16),
             pltpu.VMEM((n_tp, length, width), BF16),
+            pltpu.VMEM((n_tp, HEAD, width), BF16),
             pltpu.VMEM((length, width), F32),
             pltpu.VMEM(block, BF16),
             pltpu.VMEM((n_tp,) + block, BF16),
@@ -297,7 +347,7 @@
             pltpu.VMEM(block, BF16),
             pltpu.VMEM(block, BF16),
             pltpu.VMEM((length, width), F32),
-            dma((5,)), dma, dma, dma((n_tp,)), dma((n_tp,)), dma((n_sp,)), dma((n_sp,)),
+            dma((8,)), dma, dma, dma((n_tp,)), dma((n_tp,)), dma((n_tp,)), dma((n_tp,)), dma((n_sp,)), dma((n_sp,)),
             dma((n_sp, n_tp)), dma((n_sp, n_tp)), dma((n_sp, n_tp)), dma((n_sp, n_tp)),
             dma((n_sp,)), dma((n_sp,)),
         ],
@@ -305,9 +355,8 @@
             collective_id=0, has_side_effects=True, vmem_limit_bytes=56 << 20
         ),
     )(
-        outer_gate, inner_gate, values, conv_taps, document.astype(F32).reshape(-1, 1),
-        routes, routes.T, route_weight, norm_gain.reshape(n_tp, width),
-        mix_proj, stream, w_gate, w_up, w_down,
+        conv_taps, document.reshape(1, -1), routes.T, route_weight.T, norm_gain.reshape(1, -1),
+        outer_gate, inner_gate, values, mix_proj, stream, w_gate, w_up, w_down,
     )
 
 

time: 104 us -> 88.6 us (0.85)
  the two profiles are of different devices: /device:TPU:0 before, /device:TPU:1 now
where the time goes in v2:
time: 88.6 us; the launch traced here: 88.4 us
  Pallas kernels  86.7 us (98%)
  local copies, waits for them, and re-layouts  1.67 us (2%)
    pallas_call x1, Pallas kernels, body(): pl.pallas_call(functools.partial(kernel, n_sp, n_tp, cap), out_shape=jax....  86.7 us

profile of v2, /device:TPU:1, one launch (start us, length us, event | category | flops | bytes accessed | tf_op | source)
XLA Modules:
  0.0 88.4 jit_solution(3132293388823893181)
XLA Ops:
  0.0 86.7 %shard_map.127 = bf16[256,512]{1,0:T(8,128)(2,1)} custom-call(bf16[3,256]{1,0:T(4,128)(2,1)} %taps.1, s32[1,256]{1,0:T(1,128)} %bitcast.7, s32[2,256]{1,0:T(2,128)} %bitcast.5, f32[2,256]{1,0:T(2,128)} %bitcast.6, f32[1,2048]{1,0:T(1,128)} %bitcast.4, bf16[256,256]{1,0:T(8,128)(2,1)} %outer_hbm.1, bf16[256,256]{1,0:T(8,128)(2,1)} %inner_hbm.1, ...), custom_call_target="tpu_custom_call" | custom-call | tf_op jit(solution)/shard_map/pallas_call | solution.py:320
  86.7 1.7 %copy.15 = bf16[256,512]{1,0:T(8,128)(2,1)} copy(bf16[256,512]{1,0:T(8,128)(2,1)} %shard_map.127) | data formatting | bytes 524288
